TPU v7x, 32 devices: a whole 2x2x4 slice. The times are simulated.
32 devices in a mesh: kv: 8 (over z, x), tp: 4 (over y, core).
Axes of the slice: x: 2, y: 2, z: 4, core: 2. Of those that a mesh axis runs over, the one named last changes fastest.
Arguments:
- tokens: bfloat16 [96, 4096], P(None, 'kv'), may hold values from -210 to 210
- norm_gain: float32 [4096], P('kv'), may hold values from 0.1 to 1.9
- w_query: bfloat16 [4096, 4096], P('kv', 'tp'), may hold values from -1 to 1
- w_key: bfloat16 [4096, 4096], P('kv', 'tp'), may hold values from -2 to 2
- w_value: bfloat16 [4096, 4096], P('kv', 'tp'), may hold values from -0.09375 to 0.09375
- w_output: bfloat16 [4096, 4096], P('tp', 'kv'), may hold values from -0.09375 to 0.09375
- cache_keys: bfloat16 [4, 4096, 4096], P(None, 'kv', 'tp'), may hold values from -820 to 820
- cache_values: bfloat16 [4, 4096, 4096], P(None, 'kv', 'tp'), may hold values from -6 to 6
- map_lambda: float32 [64], P('tp'), may hold values from 0.3 to 0.8
- out_gain: float32 [4096], P('tp'), may hold values from 0.1 to 1.9
- parents: int32 [4, 24], replicated, may hold values from -1 to 22, as said below
- lengths: int32 [4], replicated, may hold values from 2048 to 4048, as said below
- accepted: int32 [4], replicated, may hold values from 0 to 24
Outputs:
- mixed: bfloat16 [96, 4096], P(None, 'kv')
- new_keys: bfloat16 [4, 4096, 4096], P(None, 'kv', 'tp')
- new_values: bfloat16 [4, 4096, 4096], P(None, 'kv', 'tp')
Inputs may be any that keep to these rules, and one draw needn't show every extreme that they name: parents[b, j] lies between -1 and j - 1. `lengths`: some sequence has exactly the largest value.
All inputs are finite; a program needn't handle non-finite values.
Results may differ from a plain program's by a relative error of at most 0.029.
Values may be sent and summed in bfloat16 or wider, within the bound.
A program may use at most 128 MiB of HBM per device.

v0:
```python
import jax
import jax.numpy as jnp
from jax import lax
from jax.sharding import PartitionSpec as P

D = 4096
HEAD = 64
QK = 32
SEQS = 4
PROP = 24


epsilon = 1e-05
masked_low = -1e30


def joined(array, axis, combine):
    everything = jax.tree.map(
        lambda part, kind: lax.all_gather(part.astype(kind), axis),
        array,
        (jnp.bfloat16, jnp.bfloat16, jnp.bfloat16),
    )

    def take(k):
        return jax.tree.map(lambda part, own: part[k].astype(own.dtype), everything, array)

    return lax.fori_loop(
        1, lax.axis_size(axis), lambda k, so_far: combine(so_far, take(k)), take(0)
    )


def ancestry(parents):
    count = parents.shape[1]
    places = jnp.arange(count, dtype=jnp.int32)
    parent_links = (parents[:, :, None] == places[None, None, :]).astype(jnp.float32)
    identity = jnp.eye(count, dtype=jnp.float32)[None]

    def extend(turn_index, reached):
        return jnp.minimum(1.0, identity + jnp.einsum("bji,bik->bjk", parent_links, reached))

    reached = lax.fori_loop(0, count, extend, jnp.broadcast_to(identity, parent_links.shape))
    return reached > 0.5


def scaled_values(values, factor, local_heads):
    shaped = values.astype(jnp.float32).reshape(values.shape[0], 2, PROP, local_heads, HEAD)
    return shaped * jnp.transpose(factor, (0, 1, 3, 2))[..., None]


def combine_blocks(earlier, later):
    max_first, total_first, values_first = earlier
    max_second, total_second, values_second = later
    largest = jnp.maximum(max_first, max_second)
    factor_first = jnp.exp(max_first - largest)
    factor_second = jnp.exp(max_second - largest)
    summed_total = total_first * factor_first + total_second * factor_second
    local_heads = max_first.shape[2]
    merged = scaled_values(values_first, factor_first, local_heads) + scaled_values(
        values_second, factor_second, local_heads
    )
    merged = merged.reshape(values_first.shape).astype(jnp.bfloat16)
    return (largest, summed_total, merged)


def local(
    tokens,
    norm_gain,
    w_query,
    w_key,
    w_value,
    w_output,
    cache_keys,
    cache_values,
    map_lambda,
    out_gain,
    parents,
    lengths,
    accepted,
):
    f32 = jnp.float32
    bf16 = jnp.bfloat16
    tokens_wide = tokens.astype(f32)
    gained = (tokens_wide * norm_gain).astype(bf16)
    partial_value = jnp.concatenate(
        [
            jnp.dot(gained, weight_part, preferred_element_type=f32)
            for weight_part in (w_query, w_key, w_value)
        ],
        axis=1,
    )
    squares = jnp.sum(tokens_wide * tokens_wide, axis=1)
    summed, total_squares = lax.psum((partial_value, squares), "kv")
    norm_factor = lax.rsqrt(total_squares / D + epsilon)
    projected = (summed * norm_factor[:, None]).astype(bf16)
    width = w_query.shape[1]
    local_heads = width // HEAD
    queries = projected[:, :width].reshape(SEQS, PROP, local_heads, 2, QK)
    keys_flat = projected[:, width : 2 * width].reshape(SEQS, PROP, width)
    values_flat = projected[:, 2 * width :].reshape(SEQS, PROP, width)
    keys_new = keys_flat.reshape(SEQS, PROP, local_heads, 2, QK)
    values_new = values_flat.reshape(SEQS, PROP, local_heads, HEAD)
    start = lengths + accepted
    score_scale = QK ** (-0.5)
    block_len = cache_keys.shape[1]
    offset = lax.axis_index("kv") * block_len
    positions = offset + jnp.arange(block_len, dtype=jnp.int32)
    visible = (positions[None, :] < start[:, None])[:, None, None, None, :]
    block_keys = cache_keys.reshape(SEQS, block_len, local_heads, 2, QK)
    block_vals = cache_values.reshape(SEQS, block_len, local_heads, HEAD)
    scores = (
        jnp.einsum("bqhmd,bkhmd->bmhqk", queries, block_keys, preferred_element_type=f32)
        * score_scale
    )
    block_max = jnp.max(jnp.where(visible, scores, masked_low), axis=-1)
    block_weight = jnp.where(visible, jnp.exp(scores - block_max[..., None]), 0.0)
    block_total = jnp.sum(block_weight, axis=-1)
    block_values = jnp.einsum(
        "bmhqk,bkhd->bmqhd", block_weight.astype(bf16), block_vals, preferred_element_type=f32
    )
    block_values = block_values.reshape(SEQS, 2, PROP, width).astype(bf16)
    cache_max, cache_total, cache_sum = joined(
        (block_max, block_total, block_values), "kv", combine_blocks
    )
    lineage = ancestry(parents)[:, None, None, :, :]
    self_scores = (
        jnp.einsum("bqhmd,bjhmd->bmhqj", queries, keys_new, preferred_element_type=f32)
        * score_scale
    )
    self_max = jnp.max(jnp.where(lineage, self_scores, masked_low), axis=-1)
    top = jnp.maximum(cache_max, self_max)
    self_weight = jnp.where(lineage, jnp.exp(self_scores - top[..., None]), 0.0)
    carried = jnp.exp(cache_max - top)
    denominator = cache_total * carried + jnp.sum(self_weight, axis=-1)
    self_values = jnp.einsum(
        "bmhqj,bjhd->bmqhd", self_weight.astype(bf16), values_new, preferred_element_type=f32
    )
    attended = (scaled_values(cache_sum, carried, local_heads) + self_values) / jnp.transpose(
        denominator, (0, 1, 3, 2)
    )[..., None]
    difference = attended[:, 0] - map_lambda[None, None, :, None] * attended[:, 1]
    gains = out_gain.reshape(local_heads, HEAD)[None, None]
    normed = (
        difference
        * lax.rsqrt(jnp.mean(difference * difference, axis=-1, keepdims=True) + epsilon)
        * gains
    )
    normed = normed.astype(bf16).reshape(SEQS * PROP, width)
    partial_out = jnp.dot(normed, w_output, preferred_element_type=f32).astype(bf16)
    partial_out = lax.optimization_barrier(partial_out).astype(f32)
    mixed = lax.psum(partial_out.astype(jnp.bfloat16), "tp").astype(jnp.float32).astype(bf16)
    relative = positions[None, :] - start[:, None]
    slots = jnp.arange(PROP, dtype=jnp.int32)
    placing = (relative[:, :, None] == slots[None, None, :]).astype(bf16)
    written = ((relative >= 0) & (relative < PROP))[:, :, None]
    moved_keys = jnp.einsum("bkj,bjf->bkf", placing, keys_flat, preferred_element_type=f32).astype(
        bf16
    )
    moved_values = jnp.einsum(
        "bkj,bjf->bkf", placing, values_flat, preferred_element_type=f32
    ).astype(bf16)
    new_keys = jnp.where(written, moved_keys, cache_keys)
    new_values = jnp.where(written, moved_values, cache_values)
    return (mixed, new_keys, new_values)


def solution(mesh):
    placed = (
        P(None, "kv"),
        P("kv"),
        P("kv", "tp"),
        P("kv", "tp"),
        P("kv", "tp"),
        P("tp", "kv"),
        P(None, "kv", "tp"),
        P(None, "kv", "tp"),
        P("tp"),
        P("tp"),
        P(),
        P(),
        P(),
    )
    return jax.shard_map(
        local,
        mesh=mesh,
        in_specs=placed,
        out_specs=(P(None, "kv"), P(None, "kv", "tp"), P(None, "kv", "tp")),
        check_vma=False,
    )
```

profile of v0, /device:TPU:1, one launch (start us, length us, event | category | flops | bytes accessed | tf_op | source)
XLA Modules:
  0.0 289.7 jit_solution(18232606850143740724)
XLA Ops:
  7.2 1.1 copy-done
  8.4 1.2 fusion.41
  9.6 1.6 fusion.43
  11.2 1.0 fusion.45
  12.2 1.1 pad_maximum_fusion
  13.4 6.2 %copy.51 = bf16[4,512,1024]{1,2,0:T(8,128)(2,1)} copy(bf16[4,512,1024]{2,1,0:T(8,128)(2,1)} %param.23) | data formatting | bytes 8388608 | tf_op args[6]
  19.6 6.2 %copy.54 = bf16[4,512,1024]{1,2,0:T(8,128)(2,1)} copy(bf16[4,512,1024]{2,1,0:T(8,128)(2,1)} %param.24) | data formatting | bytes 8388608 | tf_op args[7]
  26.0 19.0 %psum.22 = f32[96]{0:T(128)S(1)} all-reduce(f32[96]{0:T(128)S(1)} %fusion.36), channel_id=1, replica_groups=mesh['kv'=8,'tp'=4] {'kv'}, use_global_device_ids=true, to_apply=%region_2.0 | all-reduce | flops 96 | bytes 768 | tf_op jit(solution)/shard_map/psum | solution.py:92
  45.1 50.0 %all-reduce.3.cloned.1.call-done = f32[96,3072]{1,0:T(8,128)} async-done(((f32[96,3072]{1,0:T(8,128)}), f32[96,3072]{1,0:T(8,128)}) %all-reduce.3.cloned.1.call-update) | async-done | bytes 1179664 | tf_op jit(solution)/shard_map/psum | solution.py:92
  95.1 1.4 multiply_convert_fusion
  96.6 0.6 reshape.217
  97.1 4.0 %select_reduce_fusion = (f32[4,2,16,24]{3,2,1,0:T(8,128)S(1)}, f32[4,2,16,24,512]{4,3,2,1,0:T(8,128)S(1)}) fusion(pred[4,512]{1,0:T(4,128)(4,1)S(1)} %get-tuple-element.253, bf16[4,512,16,2,32]{1,4,3,2,0:T(8,128)(2,1)} %bitcast.92, bf16[4,24,16,2,32]{4,3,2,1,0:T(2,128)(2,1)S(1)} %reshape.217), kind=kOutput, calls=%fused_computation.21 | convolution fusion | flops 105378816 | bytes 10696704 | tf_op jit(solution)/shard_map/bqhmd,bkhmd->bmhqk/dot_general | solution.py:111
  101.1 2.0 fusion.13
  103.3 1.4 fusion.23
  104.9 1.3 convert_element_type.179
  106.3 5.8 %while.31 = (s32[]{:T(128)}, f32[4,24,24]{2,1,0:T(8,128)S(1)}, s32[4,24]{1,0:T(4,128)S(1)}, s32[]{:T(128)}) while((s32[]{:T(128)}, f32[4,24,24]{2,1,0:T(8,128)S(1)}, s32[4,24]{1,0:T(4,128)S(1)}, s32[]{:T(128)}) %tuple.84), condition=%wide.region_8.9_spmd.clone, body=%wide.region_7.8_spmd.clone.sunk | while | flops 120962 | bytes 41909 | solution.py:41
  112.5 0.6 reshape_reshape.6
  113.0 1.0 reshape_reshape.7
  114.1 27.7 %all-gather.1 = bf16[32,2,16,24]{3,2,1,0:T(8,128)(2,1)} all-gather(bf16[4,2,16,24]{3,2,1,0:T(8,128)(2,1)S(1)} %get-tuple-element.244), channel_id=3, replica_groups=mesh['kv'=8,'tp'=4] {'kv'}, dimensions={0}, use_global_device_ids=true | all-gather | bytes 55296 | tf_op jit(solution)/shard_map/all_gather | solution.py:19
  141.8 28.5 %all-gather = bf16[32,2,16,24]{3,2,1,0:T(8,128)(2,1)} all-gather(bf16[4,2,16,24]{3,2,1,0:T(8,128)(2,1)S(1)} %convert_element_type.168), channel_id=2, replica_groups=mesh['kv'=8,'tp'=4] {'kv'}, dimensions={0}, use_global_device_ids=true | all-gather | bytes 55296 | tf_op jit(solution)/shard_map/all_gather | solution.py:19
  170.3 1.4 slice_convert_fusion
  171.7 0.8 slice_convert_fusion.1
  172.5 3.1 %select_reduce_fusion.1 = (f32[4,2,16,24]{3,2,1,0:T(8,128)}, f32[4,2,16,24,24]{3,4,2,1,0:T(8,128)}) fusion(pred[4,24,24]{1,2,0:T(8,128)(4,1)S(1)} %copy.57, bf16[4,24,16,2,32]{4,3,2,1,0:T(2,128)(2,1)S(1)} %reshape_reshape.6, bf16[4,24,16,2,32]{4,3,2,1,0:T(2,128)(2,1)S(1)} %reshape.217), kind=kOutput, calls=%fused_computation.34 | convolution fusion | flops 4936704 | bytes 702720 | tf_op jit(solution)/shard_map/bqhmd,bjhmd->bmhqj/dot_general | solution.py:126
  175.6 2.9 convert_select_fusion
  178.5 1.0 slice_bitcast_fusion.1
  179.5 49.7 %while.30 = (s32[]{:T(128)}, f32[4,2,16,24]{3,2,1,0:T(8,128)S(1)}, f32[4,2,16,24]{3,2,1,0:T(8,128)}, bf16[4,2,24,1024]{3,2,1,0:T(8,128)(2,1)S(1)}, bf16[8,4,2,16...) while((s32[]{:T(128)}, f32[4,2,16,24]{3,2,1,0:T(8,128)S(1)}, ...), condition=%wide.region_6.7_spmd, body=%wide.region_5.6_spmd.sunk | while | flops 1210373 | bytes 7686299 | solution.py:27
  179.6 1.4 fusion.65
  181.0 1.6 fusion.66
  184.5 1.3 fusion.67
  185.8 0.8 copy.119
  186.7 1.4 fusion.65
  188.1 1.6 fusion.66
  189.7 0.5 mul.248
  191.6 1.3 fusion.67
  192.9 0.8 copy.119
  193.8 1.4 fusion.65
  195.1 1.6 fusion.66
  198.7 1.3 fusion.67
  200.0 0.8 copy.119
  200.9 1.4 fusion.65
  202.2 1.6 fusion.66
  205.8 1.3 fusion.67
  207.1 0.8 copy.119
  207.9 1.4 fusion.65
  209.3 1.6 fusion.66
  212.9 1.3 fusion.67
  214.2 0.8 copy.119
  215.0 1.4 fusion.65
  216.4 1.6 fusion.66
  220.0 1.3 fusion.67
  221.3 0.8 copy.119
  222.1 1.4 fusion.65
  223.5 1.6 fusion.66
  227.1 1.3 fusion.67
  228.4 0.8 copy.119
  229.2 0.9 fusion.47
  230.1 2.0 fusion.26
  232.1 0.9 add_bitcast_fusion
  233.5 1.6 fusion.19
  235.2 0.5 copy-done.13
  237.5 2.2 convolution_convert_fusion
  239.8 4.6 %convert_select_fusion.1 = bf16[4,512,1024]{2,1,0:T(8,128)(2,1)} fusion(bf16[4,512,1024]{2,1,0:T(8,128)(2,1)} %param.23, pred[4,512]{1,0:T(4,128)(4,1)S(1)} %get-tuple-element.252, bf16[4,24,1024]{2,1,0:T(8,128)(2,1)S(1)} %bitcast.95, s32[4,512]{1,0:T(4,128)S(1)} %broadcast_subtract_fusion), kind=kOutput, calls=%fused_computation.27 | convolution fusion | flops 104906752 | bytes 8595456 | tf_op jit(solution)/shard_map/bkj,bjf->bkf/dot_general | solution.py:155
  244.3 37.4 %all-reduce.5.cloned.1.call-done = bf16[96,512]{1,0:T(8,128)(2,1)} async-done(((bf16[96,512]{1,0:T(8,128)(2,1)}), bf16[96,512]{1,0:T(8,128)(2,1)}) %all-reduce.5.cloned.1.call-update) | async-done | bytes 98320 | tf_op jit(solution)/shard_map/psum | solution.py:150
  281.7 1.5 copy.131
  (178 shorter events, 22.2 us)
Async XLA Ops:
  7.2 1.2 copy-start
  7.2 4.0 %copy-start.6 = (bf16[96,512]{1,0:T(8,128)(2,1)S(1)}, bf16[96,512]{1,0:T(8,128)(2,1)}, u32[]{:S(2)}) copy-start(bf16[96,512]{1,0:T(8,128)(2,1)} %param.17) | copy-start | bytes 294916
  7.2 4.0 %copy-start.7 = (bf16[512,1024]{1,0:T(8,128)(2,1)S(1)}, bf16[512,1024]{1,0:T(8,128)(2,1)}, u32[]{:S(2)}) copy-start(bf16[512,1024]{1,0:T(8,128)(2,1)} %param.19) | copy-start | bytes 3145732
  7.2 87.9 %all-reduce.3.cloned.1.call-start = ((), (), s32[]{:S(2)}) async-start(), calls=%async_computation | async-start | bytes 2359296 | tf_op jit(solution)/shard_map/psum | solution.py:92
  13.4 165.1 %all-gather.4.cloned.1.call-start = ((), (), s32[]{:S(2)}) async-start(), calls=%async_computation.1 | async-start | bytes 3538944 | tf_op jit(solution)/shard_map/all_gather | solution.py:19
  19.6 6.2 %copy-start.14 = (s32[4]{0:T(128)S(1)}, s32[4]{0:T(128)}, u32[]{:S(2)}) copy-start(s32[4]{0:T(128)} %param.28) | copy-start | bytes 52
  19.6 6.2 %copy-start.15 = (s32[4]{0:T(128)S(1)}, s32[4]{0:T(128)}, u32[]{:S(2)}) copy-start(s32[4]{0:T(128)} %param.29) | copy-start | bytes 52
  96.6 15.9 %copy-start.4 = (bf16[96,1024]{1,0:T(8,128)(2,1)}, bf16[96,1024]{1,0:T(8,128)(2,1)S(1)}, u32[]{:S(2)}) copy-start(bf16[96,1024]{1,0:T(8,128)(2,1)S(1)} %get-tuple-element.250) | copy-start | bytes 589828
  101.1 2.2 copy-start.3
  104.7 1.6 copy-start.9
  104.7 7.5 %copy-start.12 = (f32[16]{0:T(128)S(1)}, f32[16]{0:T(128)}, u32[]{:S(2)}) copy-start(f32[16]{0:T(128)} %param.25) | copy-start | bytes 196
  106.2 175.4 %all-reduce.5.cloned.1.call-start = ((), (), s32[]{:S(2)}) async-start(), calls=%async_computation.2 | async-start | bytes 196608 | tf_op jit(solution)/shard_map/psum | solution.py:150
  112.2 66.3 %copy-start.10 = (pred[4,24,24]{1,2,0:T(8,128)(4,1)}, pred[4,24,24]{1,2,0:T(8,128)(4,1)S(1)}, u32[]{:S(2)}) copy-start(pred[4,24,24]{1,2,0:T(8,128)(4,1)S(1)} %copy.57) | copy-start | bytes 6916
  114.1 61.6 %copy-start.2 = (bf16[4,512,1024]{2,1,0:T(8,128)(2,1)S(1)}, bf16[4,512,1024]{2,1,0:T(8,128)(2,1)}, u32[]{:S(2)}) copy-start(bf16[4,512,1024]{2,1,0:T(8,128)(2,1)} %param.24) | copy-start | bytes 12582916
  229.2 4.3 %copy-start.8 = (bf16[4,24,16,64]{3,2,1,0:T(8,128)(2,1)S(1)}, bf16[4,24,16,64]{3,2,1,0:T(8,128)(2,1)}, u32[]{:S(2)}) copy-start(bf16[4,24,16,64]{3,2,1,0:T(8,128)(2,1)} %reshape_reshape.7) | copy-start | bytes 589828
  235.1 0.7 copy-start.13
  236.2 1.3 copy-start.11
  236.6 3.1 %copy-start.5 = (bf16[96,1024]{1,0:T(8,128)(2,1)S(1)}, bf16[96,1024]{1,0:T(8,128)(2,1)}, u32[]{:S(2)}) copy-start(bf16[96,1024]{1,0:T(8,128)(2,1)} %copy-done.4) | copy-start | bytes 589828
  239.7 43.5 %copy-start.1 = (bf16[512,1024]{1,0:T(8,128)(2,1)S(1)}, bf16[512,1024]{1,0:T(8,128)(2,1)}, u32[]{:S(2)}) copy-start(bf16[512,1024]{1,0:T(8,128)(2,1)} %param.21) | copy-start | bytes 3145732
Sparse Core Ops, SparseCore 0:
  13.5 81.5 all-reduce.2
  106.4 63.2 all-gather.3
  239.9 41.7 all-reduce.4
where the time goes:
time: 294 us; the launch traced here: 290 us
  waiting for transfers between devices  87.4 us (30%)
  blocking collectives  75.3 us (26%)
  local copies, waits for them, and re-layouts  42.7 us (15%)
  other arithmetic  40.8 us (14%)
  matrix products  28.4 us (10%)
  between operations  14.1 us (5%)
    all_gather x2, blocking collectives, joined(): lax.all_gather(part.astype(kind), axis)  56.3 us
    psum x1, waiting for transfers between devices, local(): summed, total_squares = lax.psum((partial_value, squares), 'kv')  50 us
    psum x1, waiting for transfers between devices, local(): lax.psum(partial_out.astype(jnp.bfloat16), 'tp').astype(jnp.float32)  37.4 us
    transpose x15, other arithmetic, scaled_values(): return shaped * jnp.transpose(factor, (0, 1, 3, 2))[..., None]  21.6 us
    psum x1, blocking collectives, local(): summed, total_squares = lax.psum((partial_value, squares), 'kv')  19 us
    unnamed x35, local copies, waits for them, and re-layouts  15.9 us
    mul x28, local copies, waits for them, and re-layouts, scaled_values(): return shaped * jnp.transpose(factor, (0, 1, 3, 2))[..., None]  12.8 us
    convert_element_type x7, other arithmetic, combine_blocks(): merged = merged.reshape(values_first.shape).astype(jnp.bfloat16)  8.9 us
  transfers between devices with their start and end apart: 3, of which 2 were waited for; matrix products, arithmetic and copies ran while one was open for 11% of the time, Pallas kernels for 0%

commit v1 on v0

v1 whole, which is shorter than its diff:
```python
import functools

import jax
import jax.numpy as jnp
from jax import lax
from jax.experimental import pallas as pl
from jax.experimental.pallas import tpu as pltpu
from jax.sharding import PartitionSpec as P

HEAD = 64
QK = 32
LANES = 128
epsilon = 1e-05
masked_low = -1e30
MESH = pl.DeviceIdType.MESH
f32 = jnp.float32
bf16 = jnp.bfloat16


def iota(shape, dim):
    return lax.broadcasted_iota(jnp.int32, shape, dim)


def greet(axes):
    barrier = pltpu.get_barrier_semaphore()
    count = 0
    for axis, n in axes:
        me = lax.axis_index(axis)
        for k in range(1, n):
            pl.semaphore_signal(
                barrier, inc=1, device_id={axis: lax.rem(me + k, n)}, device_id_type=MESH
            )
            count += 1
    return barrier, count


def remote(src, dst, send_sem, recv_sem, axis, to):
    return pltpu.make_async_remote_copy(
        src_ref=src,
        dst_ref=dst,
        send_sem=send_sem,
        recv_sem=recv_sem,
        device_id={axis: to},
        device_id_type=MESH,
    )


def project_kernel(
    n, cols, features, tok_ref, gain_ref, wq_ref, wk_ref, wv_ref, out_ref,
    send, recv, sq_send, sq_recv, s_send, s_recv, q_send, q_recv, g_send, g_recv,
):
    me = lax.axis_index("kv")
    groups = n // cols
    rows = tok_ref.shape[0]
    part = rows // groups
    barrier, count = greet((("kv", n),))
    wide = tok_ref[...].astype(f32)
    gained = (wide * gain_ref[...]).astype(bf16)
    square = jnp.sum(wide * wide, axis=1, keepdims=True)
    diagonal = iota((rows, LANES), 0) == iota((rows, LANES), 1)
    as_row = jnp.sum(jnp.where(diagonal, square, 0.0), axis=0, keepdims=True)
    sq_send[...] = jnp.broadcast_to(as_row, sq_send.shape)
    for i, ref in enumerate((wq_ref, wk_ref, wv_ref)):
        product = jnp.dot(gained, ref[...], preferred_element_type=f32)
        for c in range(cols):
            for r in range(groups):
                send[c * groups + r, :, i * LANES : (i + 1) * LANES] = product[
                    r * part : (r + 1) * part, c * LANES : (c + 1) * LANES
                ].astype(bf16)
    pl.semaphore_wait(barrier, count)
    copies = []
    for k in range(1, n):
        to = lax.rem(me + k, n)
        copies.append(remote(sq_send, sq_recv.at[k], q_send.at[k], q_recv.at[k], "kv", to))
        copies.append(remote(send.at[to], recv.at[k], s_send.at[k], s_recv.at[k], "kv", to))
    for copy in copies:
        copy.start()
    total = send[me].astype(f32)
    squares = sq_send[...]
    for k in range(1, n):
        copies[2 * k - 2].wait()
        squares = squares + sq_recv[k]
    for k in range(1, n):
        copies[2 * k - 1].wait()
        total = total + recv[k].astype(f32)
    first = lax.rem(me, groups) * part
    picked = iota((part, LANES), 0) + first == iota((part, LANES), 1)
    mean = jnp.sum(jnp.where(picked, squares[0:1], 0.0), axis=1, keepdims=True) / features
    out_ref[me] = (total * lax.rsqrt(mean + epsilon)).astype(bf16)
    copies = []
    for k in range(1, n):
        to = lax.rem(me + k, n)
        copies.append(remote(out_ref.at[me], out_ref.at[me], g_send.at[k], g_recv.at[k], "kv", to))
    for copy in copies:
        copy.start()
    for copy in copies:
        copy.wait()


def cache_kernel(
    groups, prop, rel_ref, ga_ref, keys_hbm, vals_hbm, nk_hbm, nv_hbm, bv_ref, st_ref,
    kbuf, vbuf, k_in, v_in, k_out, v_out,
):
    seqs, length, width = kbuf.shape
    cols = width // LANES
    per = seqs // groups
    both = 2 * prop
    loads = []
    for b in range(seqs):
        loads.append(
            (
                pltpu.make_async_copy(keys_hbm.at[b], kbuf.at[b], k_in.at[b]),
                pltpu.make_async_copy(vals_hbm.at[b], vbuf.at[b], v_in.at[b]),
            )
        )
        loads[b][0].start()
        loads[b][1].start()
    st_ref[...] = jnp.zeros_like(st_ref)
    stores = []
    window = 48
    lane = iota((1, LANES), 1)
    wide_lane = iota((1, 2 * LANES), 1)
    scale = QK ** (-0.5)
    for b in range(seqs):
        r, inner = b // per, b % per
        begin = inner * prop
        rel = rel_ref[b]

        def fresh(which):
            return jnp.concatenate(
                [
                    ga_ref[c * groups + r, begin : begin + prop, which * LANES : (which + 1) * LANES]
                    for c in range(cols)
                ],
                axis=1,
            )

        base = jnp.clip((rel // 16) * 16, 0, length - window)
        at = pl.ds(pl.multiple_of(base, 16), window)
        slot = iota((window, prop), 0) + base - rel
        placing = (slot == iota((window, prop), 1)).astype(bf16)
        slot_col = iota((window, 1), 0) + base - rel
        inside = (slot_col >= 0) & (slot_col < prop)
        for which, buf, pos in ((1, kbuf, 0), (2, vbuf, 1)):
            loads[b][pos].wait()
            moved = jnp.dot(placing, fresh(which), preferred_element_type=f32)
            old = buf[b, at, :].astype(f32)
            buf[b, at, :] = jnp.where(inside, moved, old).astype(bf16)
        stores.append(pltpu.make_async_copy(kbuf.at[b], nk_hbm.at[b], k_out.at[b]))
        stores.append(pltpu.make_async_copy(vbuf.at[b], nv_hbm.at[b], v_out.at[b]))
        stores[-2].start()
        stores[-1].start()
        queries = fresh(0)
        visible = iota((1, length), 1) < rel
        for g in range(width // (2 * LANES)):
            span = slice(g * 2 * LANES, (g + 1) * 2 * LANES)
            part = queries[:, span].astype(f32)
            spread = jnp.concatenate(
                [jnp.where(wide_lane // QK == i, part, 0.0) for i in range(2 * LANES // QK)], axis=0
            ).astype(bf16)
            scores = lax.dot_general(
                spread, kbuf[b, :, span], (((1,), (1,)), ((), ())), preferred_element_type=f32
            )
            scores = jnp.where(visible, scores * scale, masked_low)
            largest = jnp.max(scores, axis=1, keepdims=True)
            weight = jnp.where(visible, jnp.exp(scores - largest), 0.0)
            total = jnp.sum(weight, axis=1, keepdims=True)
            summed = jnp.dot(weight.astype(bf16), vbuf[b, :, span], preferred_element_type=f32)
            merged = jnp.zeros((both, 2 * LANES), f32)
            for h in range(2 * LANES // HEAD):
                piece = slice(h * both, (h + 1) * both)
                merged = jnp.where(wide_lane // HEAD == h, summed[piece], merged)
                c = g * 2 + h // 2
                first = inner * 4 + h % 2
                stat = st_ref[c, r]
                stat = jnp.where(lane == first, largest[piece], stat)
                st_ref[c, r] = jnp.where(lane == first + 2, total[piece], stat)
            merged = merged.astype(bf16)
            for half in range(2):
                bv_ref[g * 2 + half, r, inner * both : (inner + 1) * both, :] = merged[
                    :, half * LANES : (half + 1) * LANES
                ]
    for copy in stores:
        copy.wait()


def merge_kernel(
    n, t, cols, seqs, prop, parent_ref, lam_ref, gain_ref, ga_ref, bv_ref, st_ref, wo_ref, out_ref,
    bv_recv, st_recv, norm_all, out_part, out_recv,
    b_send, b_recv, s_send, s_recv, g_send, g_recv, t_send, t_recv,
):
    me = lax.axis_index("kv")
    mine = lax.axis_index("tp")
    groups = n // cols
    per = seqs // groups
    part = per * prop
    both = 2 * prop
    barrier, count = greet((("kv", n), ("tp", t)))
    pl.semaphore_wait(barrier, count)
    copies = []
    for k in range(1, n):
        to = lax.rem(me + k, n)
        c, r = to // groups, lax.rem(to, groups)
        copies.append(remote(st_ref.at[c, r], st_recv.at[k], s_send.at[k], s_recv.at[k], "kv", to))
        copies.append(remote(bv_ref.at[c, r], bv_recv.at[k], b_send.at[k], b_recv.at[k], "kv", to))
    for copy in copies:
        copy.start()
    col, row = me // groups, lax.rem(me, groups)
    lane = iota((1, LANES), 1)
    scale = QK ** (-0.5)
    shape = (part, part)
    target = parent_ref[...] + (iota((part, 1), 0) // prop) * prop
    link = (parent_ref[...] >= 0) & (target == iota(shape, 1))
    eye = iota(shape, 0) == iota(shape, 1)
    reach = jnp.where(link | eye, 1.0, 0.0)
    power = 1
    while power < prop:
        reach = jnp.minimum(
            jnp.dot(reach.astype(bf16), reach.astype(bf16), preferred_element_type=f32), 1.0
        )
        power *= 2
    lineage = jnp.concatenate([reach] * 4, axis=0) > 0.5
    own = ga_ref[me]
    query = own[:, :LANES].astype(f32)
    spread = jnp.concatenate(
        [jnp.where(lane // QK == i, query, 0.0) for i in range(4)], axis=0
    ).astype(bf16)
    scores = lax.dot_general(
        spread, own[:, LANES : 2 * LANES], (((1,), (1,)), ((), ())), preferred_element_type=f32
    )
    scores = jnp.where(lineage, scores * scale, masked_low)
    top = jnp.max(scores, axis=1, keepdims=True)
    weight = jnp.where(lineage, jnp.exp(scores - top), 0.0)
    total = jnp.sum(weight, axis=1, keepdims=True)
    summed = jnp.dot(weight.astype(bf16), own[:, 2 * LANES :], preferred_element_type=f32)
    low = lane < HEAD

    def laid(array):
        pieces = []
        for b in range(per):
            for m in range(2):
                s0 = slice(m * part + b * prop, m * part + (b + 1) * prop)
                s1 = slice((2 + m) * part + b * prop, (2 + m) * part + (b + 1) * prop)
                pieces.append(jnp.where(low, array[s0], array[s1]))
        return jnp.concatenate(pieces, axis=0)

    tops = [laid(top)]
    totals = [laid(total)]
    sums = [laid(summed)]

    def take(stats, values):
        for which, into in ((0, tops), (2, totals)):
            into.append(
                jnp.concatenate(
                    [
                        jnp.where(
                            low,
                            stats[:, b * 4 + which : b * 4 + which + 1],
                            stats[:, b * 4 + which + 1 : b * 4 + which + 2],
                        )
                        for b in range(per)
                    ],
                    axis=0,
                )
            )
        sums.append(values.astype(f32))

    take(st_ref[col, row], bv_ref[col, row])
    for copy in copies:
        copy.wait()
    for k in range(1, n):
        take(st_recv[k], bv_recv[k])
    highest = functools.reduce(jnp.maximum, tops)
    denominator = jnp.zeros_like(highest)
    numerator = jnp.zeros_like(highest)
    for a, b, c in zip(tops, totals, sums):
        factor = jnp.exp(a - highest)
        denominator = denominator + b * factor
        numerator = numerator + c * factor
    attended = numerator / denominator
    lam = lam_ref[pl.ds(col, 1), :]
    gain = gain_ref[pl.ds(col, 1), :]
    difference = jnp.concatenate(
        [
            attended[b * both : b * both + prop] - lam * attended[b * both + prop : (b + 1) * both]
            for b in range(per)
        ],
        axis=0,
    )
    squared = difference * difference
    one = jnp.sum(jnp.where(low, squared, 0.0), axis=1, keepdims=True)
    two = jnp.sum(jnp.where(low, 0.0, squared), axis=1, keepdims=True)
    mean = jnp.where(low, one, two) / HEAD
    norm_all[me] = (difference * lax.rsqrt(mean + epsilon) * gain).astype(bf16)
    copies = []
    for k in range(1, n):
        to = lax.rem(me + k, n)
        copies.append(
            remote(norm_all.at[me], norm_all.at[me], g_send.at[k], g_recv.at[k], "kv", to)
        )
    for copy in copies:
        copy.start()
    for copy in copies:
        copy.wait()
    normed = jnp.concatenate(
        [
            jnp.concatenate([norm_all[c * groups + r] for r in range(groups)], axis=0)
            for c in range(cols)
        ],
        axis=1,
    )
    out_part[...] = jnp.dot(normed, wo_ref[...], preferred_element_type=f32).astype(bf16)
    copies = []
    for k in range(1, t):
        to = lax.rem(mine + k, t)
        copies.append(remote(out_part, out_recv.at[k], t_send.at[k], t_recv.at[k], "tp", to))
    for copy in copies:
        copy.start()
    mixed = out_part[...].astype(f32)
    for k in range(1, t):
        copies[k - 1].wait()
        mixed = mixed + out_recv[k].astype(f32)
    out_ref[...] = mixed.astype(bf16)


def local(
    n, t, tokens, norm_gain, w_query, w_key, w_value, w_output, cache_keys, cache_values,
    map_lambda, out_gain, parents, lengths, accepted,
):
    rows, depth = tokens.shape
    seqs, length, width = cache_keys.shape
    prop = rows // seqs
    both = 2 * prop
    cols = min(n, width // LANES)
    groups = n // cols
    part = rows // groups
    per = seqs // groups
    vmem = pl.BlockSpec(memory_space=pltpu.VMEM)
    smem = pl.BlockSpec(memory_space=pltpu.SMEM)
    hbm = pl.BlockSpec(memory_space=pl.ANY)
    dma = pltpu.SemaphoreType.DMA
    gathered = pl.pallas_call(
        functools.partial(project_kernel, n, cols, depth * n),
        name="project",
        out_shape=jax.ShapeDtypeStruct((n, part, 3 * LANES), bf16),
        in_specs=[vmem] * 5,
        out_specs=vmem,
        scratch_shapes=[
            pltpu.VMEM((n, part, 3 * LANES), bf16),
            pltpu.VMEM((n, part, 3 * LANES), bf16),
            pltpu.VMEM((8, LANES), f32),
            pltpu.VMEM((n, 8, LANES), f32),
        ]
        + [dma((n,))] * 6,
        compiler_params=pltpu.CompilerParams(collective_id=0, has_side_effects=True),
    )(tokens, norm_gain[None], w_query, w_key, w_value)
    start = lengths + accepted
    relative = (start - lax.axis_index("kv") * length).astype(jnp.int32)
    new_keys, new_values, block_values, stats = pl.pallas_call(
        functools.partial(cache_kernel, groups, prop),
        name="cache",
        out_shape=(
            jax.ShapeDtypeStruct(cache_keys.shape, bf16),
            jax.ShapeDtypeStruct(cache_values.shape, bf16),
            jax.ShapeDtypeStruct((cols, groups, per * both, LANES), bf16),
            jax.ShapeDtypeStruct((cols, groups, both, LANES), f32),
        ),
        in_specs=[smem, vmem, hbm, hbm],
        out_specs=(hbm, hbm, vmem, vmem),
        scratch_shapes=[
            pltpu.VMEM(cache_keys.shape, bf16),
            pltpu.VMEM(cache_values.shape, bf16),
        ]
        + [dma((seqs,))] * 4,
    )(relative, gathered, cache_keys, cache_values)
    first = lax.rem(lax.axis_index("kv"), groups) * per
    own_parents = lax.dynamic_slice_in_dim(parents, first, per, 0).reshape(part, 1)
    mixed = pl.pallas_call(
        functools.partial(merge_kernel, n, t, cols, seqs, prop),
        name="merge",
        out_shape=jax.ShapeDtypeStruct((rows, w_output.shape[1]), bf16),
        in_specs=[vmem] * 7,
        out_specs=vmem,
        scratch_shapes=[
            pltpu.VMEM((n, per * both, LANES), bf16),
            pltpu.VMEM((n, both, LANES), f32),
            pltpu.VMEM((n, part, LANES), bf16),
            pltpu.VMEM((rows, w_output.shape[1]), bf16),
            pltpu.VMEM((t, rows, w_output.shape[1]), bf16),
        ]
        + [dma((n,))] * 6
        + [dma((t,))] * 2,
        compiler_params=pltpu.CompilerParams(collective_id=1, has_side_effects=True),
    )(
        own_parents,
        jnp.repeat(map_lambda, HEAD).reshape(cols, LANES),
        out_gain.reshape(cols, LANES),
        gathered,
        block_values,
        stats,
        w_output,
    )
    return (mixed, new_keys, new_values)


def solution(mesh):
    placed = (
        P(None, "kv"),
        P("kv"),
        P("kv", "tp"),
        P("kv", "tp"),
        P("kv", "tp"),
        P("tp", "kv"),
        P(None, "kv", "tp"),
        P(None, "kv", "tp"),
        P("tp"),
        P("tp"),
        P(),
        P(),
        P(),
    )
    return jax.shard_map(
        functools.partial(local, mesh.shape["kv"], mesh.shape["tp"]),
        mesh=mesh,
        in_specs=placed,
        out_specs=(P(None, "kv"), P(None, "kv", "tp"), P(None, "kv", "tp")),
        check_vma=False,
    )
```

time: 294 us -> 87.4 us (0.30); the launches traced: 290 us -> 87.2 us
  waiting for transfers between devices: 87.4 us -> 0 us
  Pallas kernels: 0 us -> 80.9 us
  blocking collectives: 75.3 us -> 0 us
  other arithmetic: 40.8 us -> 1.2 us
  local copies, waits for them, and re-layouts: 42.7 us -> 4.42 us
  matrix products: 28.4 us -> 0 us
  between operations: 14.1 us -> 0.66 us
    psum x2 -> x0, waiting for transfers between devices: 87.4 us -> none  [the longest x1 50 us: local(): summed, total_squares = lax.psum((partial_value, squares), 'kv')]
    pallas_call x0 -> x3, Pallas kernels: none -> 80.9 us  [the longest x1 37.8 us: local(): pl.pallas_call(functools.partial(merge_kernel, n, t, cols, seqs, prop), n...]
    all_gather x2 -> x0, blocking collectives: 56.3 us -> none  [joined(): lax.all_gather(part.astype(kind), axis)]
    dot_general x34 -> x0, matrix products: 28.4 us -> none  [the longest x24 4.95 us: extend(): jnp.einsum('bji,bik->bjk', parent_links, reached)]
    transpose x16 -> x0, other arithmetic: 22.5 us -> none  [the longest x15 21.6 us: scaled_values(): return shaped * jnp.transpose(factor, (0, 1, 3, 2))[..., None]]
    psum x1 -> x0, blocking collectives: 19 us -> none  [local(): summed, total_squares = lax.psum((partial_value, squares), 'kv')]
    convert_element_type x13 -> x0, other arithmetic: 14.5 us -> none  [the longest x7 8.9 us: combine_blocks(): merged = merged.reshape(values_first.shape).astype(jnp.bfloat16)]
    unnamed x35 -> x1, local copies, waits for them, and re-layouts: 15.9 us -> 1.54 us
  transfers between devices with their start and end apart: 3 -> 0, of which waited for: 2 -> 0; matrix products, arithmetic and copies ran while one was open for 11% -> 0% of each run, Pallas kernels for 0% -> 0%
where the time goes in v1:
time: 87.4 us; the launch traced here: 87.2 us
  Pallas kernels  80.9 us (93%)
  local copies, waits for them, and re-layouts  4.42 us (5%)
  other arithmetic  1.2 us (1%)
    pallas_call x1, Pallas kernels, local(): pl.pallas_call(functools.partial(merge_kernel, n, t, cols, seqs, prop), n...  37.8 us
    pallas_call x1, Pallas kernels, local(): pl.pallas_call(functools.partial(project_kernel, n, cols, depth * n), nam...  33.5 us
    pallas_call x1, Pallas kernels, local(): pl.pallas_call(functools.partial(cache_kernel, groups, prop), name='cache...  9.6 us

profile of v1, /device:TPU:1, one launch (start us, length us, event | category | flops | bytes accessed | tf_op | source)
XLA Modules:
  0.0 87.2 jit_solution(14252336181548732702)
XLA Ops:
  0.6 1.2 %add_subtract_fusion.rel_ref = s32[4]{0:T(128)} fusion(s32[4]{0:T(128)} %param.24, s32[4]{0:T(128)} %param.25, s32[]{:T(128)S(6)} %mul.4), kind=kLoop, calls=%fused_computation | loop fusion | flops 8 | bytes 52 | tf_op jit(solution)/shard_map/sub | solution.py:358
  1.8 0.7 broadcast_in_dim.10
  2.6 0.1 broadcast_in_dim.11
  2.6 0.7 broadcast_in_dim.12.lam_ref
  3.3 1.4 %reshape.16.parent_ref = s32[96,1]{1,0:T(8,128)} reshape(s32[4,24]{1,0:T(4,128)} %param.23) | data formatting | bytes 768 | tf_op jit(solution)/shard_map/reshape | solution.py:377
  4.7 33.5 %project.1.ga_ref = bf16[8,96,384]{2,1,0:T(8,128)(2,1)} custom-call(bf16[96,512]{1,0:T(8,128)(2,1)} %tok_ref.1, f32[1,512]{1,0:T(1,128)} %bitcast.3, bf16[512,1024]{1,0:T(8,128)(2,1)} %wq_ref.1, bf16[512,1024]{1,0:T(8,128)(2,1)} %wk_ref.1, bf16[512,1024]{1,0:T(8,128)(2,1)} %wv_ref.1), custom_call_target="tpu_custom_call" | custom-call | tf_op jit(solution)/shard_map/project/pallas_call | solution.py:342
  38.2 9.6 %cache.1 = (bf16[4,512,1024]{2,1,0:T(8,128)(2,1)}, bf16[4,512,1024]{2,1,0:T(8,128)(2,1)}, bf16[8,1,192,128]{3,2,1,0:T(8,128)(2,1)}, f32[8,1,48,128]{3,2,1,0:T(8,128)}) custom-call(s32[4]{0:T(128)} %add_subtract_fusion.rel_ref, bf16[8,96,384]{2,1,0:T(8,128)(2,1)} %project.1.ga_ref, bf16[4,512,1024]{2,1,0:T(8,128)(2,1)} %keys_hbm.1, bf16[4,512,1024]{2,1,0:T(8,128)(2,1)} %vals_hbm.1), custom_call_target="tpu_custom_call" | custom-call | tf_op jit(solution)/shard_map/cache/pallas_call | solution.py:359
  47.8 37.8 %merge.1 = bf16[96,512]{1,0:T(8,128)(2,1)} custom-call(s32[96,1]{1,0:T(8,128)} %reshape.16.parent_ref, f32[8,128]{1,0:T(8,128)} %broadcast_in_dim.12.lam_ref, f32[8,128]{1,0:T(8,128)} %bitcast.2, bf16[8,96,384]{2,1,0:T(8,128)(2,1)} %project.1.ga_ref, bf16[8,1,192,128]{3,2,1,0:T(8,128)(2,1)} %get-tuple-element.7.bv_ref, ...), custom_call_target="tpu_custom_call" | custom-call | tf_op jit(solution)/shard_map/merge/pallas_call | solution.py:378
  85.7 1.5 %copy.19 = bf16[96,512]{1,0:T(8,128)(2,1)} copy(bf16[96,512]{1,0:T(8,128)(2,1)} %merge.1) | data formatting | bytes 196608

commit v2 on v1

v2 whole, which is shorter than its diff:
```python
import functools

import jax
import jax.numpy as jnp
from jax import lax
from jax.experimental import pallas as pl
from jax.experimental.pallas import tpu as pltpu
from jax.sharding import PartitionSpec as P

HEAD = 64
QK = 32
LANES = 128
epsilon = 1e-05
masked_low = -1e30
MESH = pl.DeviceIdType.MESH
f32 = jnp.float32
bf16 = jnp.bfloat16


def iota(shape, dim):
    return lax.broadcasted_iota(jnp.int32, shape, dim)


def greet(axes):
    barrier = pltpu.get_barrier_semaphore()
    count = 0
    for axis, n in axes:
        me = lax.axis_index(axis)
        for k in range(1, n):
            pl.semaphore_signal(
                barrier, inc=1, device_id={axis: lax.rem(me + k, n)}, device_id_type=MESH
            )
            count += 1
    return barrier, count


def remote(src, dst, send_sem, recv_sem, axis, to):
    return pltpu.make_async_remote_copy(
        src_ref=src,
        dst_ref=dst,
        send_sem=send_sem,
        recv_sem=recv_sem,
        device_id={axis: to},
        device_id_type=MESH,
    )


def main_kernel(
    n, t, cols, seqs, prop, features,
    tok_ref, gain_ref, lam_ref, out_gain_ref, parent_ref, len_ref, acc_ref,
    wq_hbm, wk_hbm, wv_hbm, wo_hbm, keys_hbm, vals_hbm,
    out_ref, kv_ref,
    wbuf, wo_buf, kbuf, vbuf, q_part, q_recv, q_all, kv_part, kv_recv, sq_part, sq_recv,
    bv, bv_recv, st, st_part, st_recv, norm_all, out_part, out_recv,
    w_in, k_in, v_in, sq_s, sq_r, q_s, q_r, qa_s, qa_r, kv_s, kv_r, ka_s, ka_r,
    b_s, b_r, st_s, st_r, g_s, g_r, t_s, t_r,
):
    me = lax.axis_index("kv")
    mine = lax.axis_index("tp")
    groups = n // cols
    rows = tok_ref.shape[0]
    part = rows // groups
    per = seqs // groups
    both = 2 * prop
    _, length, width = kbuf.shape
    scale = QK ** (-0.5)
    peers = [lax.rem(me + k, n) for k in range(1, n)]
    barrier, count = greet((("kv", n), ("tp", t)))
    weights = [
        pltpu.make_async_copy(src, dst, w_in.at[i])
        for i, (src, dst) in enumerate(
            ((wq_hbm, wbuf.at[0]), (wk_hbm, wbuf.at[1]), (wv_hbm, wbuf.at[2]), (wo_hbm, wo_buf))
        )
    ]
    loads = []
    for b in range(seqs):
        loads.append(pltpu.make_async_copy(keys_hbm.at[b], kbuf.at[b], k_in.at[b]))
        loads.append(pltpu.make_async_copy(vals_hbm.at[b], vbuf.at[b], v_in.at[b]))
    for copy in weights + loads:
        copy.start()

    wide = tok_ref[...].astype(f32)
    square = jnp.sum(wide * wide, axis=1, keepdims=True)
    diagonal = iota((rows, LANES), 0) == iota((rows, LANES), 1)
    as_row = jnp.sum(jnp.where(diagonal, square, 0.0), axis=0, keepdims=True)
    sq_part[...] = jnp.broadcast_to(as_row, sq_part.shape)
    gained = (wide * gain_ref[...]).astype(bf16)

    def products(which, into, at):
        weights[which].wait()
        product = jnp.dot(gained, wbuf[which], preferred_element_type=f32)
        for c in range(cols):
            for r in range(groups):
                into[c * groups + r, :, at : at + LANES] = product[
                    r * part : (r + 1) * part, c * LANES : (c + 1) * LANES
                ].astype(bf16)

    products(0, q_part, 0)
    pl.semaphore_wait(barrier, count)
    sq_copies, q_copies = [], []
    for k, to in enumerate(peers):
        sq_copies.append(remote(sq_part, sq_recv.at[k], sq_s.at[k], sq_r.at[k], "kv", to))
        q_copies.append(remote(q_part.at[to], q_recv.at[k], q_s.at[k], q_r.at[k], "kv", to))
    for copy in sq_copies + q_copies:
        copy.start()
    products(1, kv_part, 0)
    products(2, kv_part, LANES)
    squares = sq_part[...]
    for k in range(n - 1):
        sq_copies[k].wait()
        squares = squares + sq_recv[k]
    first = lax.rem(me, groups) * part
    picked = iota((part, LANES), 0) + first == iota((part, LANES), 1)
    mean = jnp.sum(jnp.where(picked, squares[0:1], 0.0), axis=1, keepdims=True) / features
    factor = lax.rsqrt(mean + epsilon)
    total = q_part[me].astype(f32)
    for k in range(n - 1):
        q_copies[k].wait()
        total = total + q_recv[k].astype(f32)
    q_all[me] = (total * factor).astype(bf16)
    gathers, kv_copies = [], []
    for k, to in enumerate(peers):
        gathers.append(remote(q_all.at[me], q_all.at[me], qa_s.at[k], qa_r.at[k], "kv", to))
        kv_copies.append(remote(kv_part.at[to], kv_recv.at[k], kv_s.at[k], kv_r.at[k], "kv", to))
    for copy in gathers + kv_copies:
        copy.start()

    lane = iota((1, LANES), 1)
    low = lane < HEAD
    own_first = lax.rem(me, groups) * per
    small_eye = iota((prop, prop), 0) == iota((prop, prop), 1)
    parent_rows = []
    for b in range(per):
        line = parent_ref[pl.ds(own_first + b, 1), :]
        parent_rows.append(
            jnp.sum(jnp.where(small_eye, line, 0), axis=1, keepdims=True)
        )
    parent = jnp.concatenate(parent_rows, axis=0)
    shape = (part, part)
    target = jnp.concatenate([p + b * prop for b, p in enumerate(parent_rows)], axis=0)
    link = (parent >= 0) & (target == iota(shape, 1))
    reach = jnp.where(link | (iota(shape, 0) == iota(shape, 1)), 1.0, 0.0)
    power = 1
    while power < prop:
        reach = jnp.minimum(
            jnp.dot(reach.astype(bf16), reach.astype(bf16), preferred_element_type=f32), 1.0
        )
        power *= 2
    lineage = jnp.concatenate([reach] * 4, axis=0) > 0.5
    st[...] = jnp.zeros_like(st)

    for copy in gathers:
        copy.wait()
    wide_lane = iota((1, 2 * LANES), 1)
    b_copies = []
    pieces = seqs if groups == 1 else 1
    tall = per * both // pieces

    def send_piece(piece):
        for k, to in enumerate(peers):
            c, r = to // groups, lax.rem(to, groups)
            span = pl.ds(piece * tall, tall)
            copy = remote(
                bv.at[c, r, span], bv_recv.at[k, span], b_s.at[k, piece], b_r.at[k, piece], "kv", to
            )
            copy.start()
            b_copies.append(copy)

    for b in range(seqs):
        r, inner = b // per, b % per
        begin = inner * prop
        rel = len_ref[b] + acc_ref[b] - me * length
        visible = iota((1, length), 1) < rel
        loads[2 * b].wait()
        loads[2 * b + 1].wait()
        for g in range(width // (2 * LANES)):
            span = slice(g * 2 * LANES, (g + 1) * 2 * LANES)
            query = jnp.concatenate(
                [
                    q_all[c * groups + r].astype(f32)[begin : begin + prop]
                    for c in (2 * g, 2 * g + 1)
                ],
                axis=1,
            )
            spread = jnp.concatenate(
                [jnp.where(wide_lane // QK == i, query, 0.0) for i in range(2 * LANES // QK)],
                axis=0,
            ).astype(bf16)
            scores = lax.dot_general(
                spread, kbuf[b, :, span], (((1,), (1,)), ((), ())), preferred_element_type=f32
            )
            scores = jnp.where(visible, scores * scale, masked_low)
            largest = jnp.max(scores, axis=1, keepdims=True)
            weight = jnp.where(visible, jnp.exp(scores - largest), 0.0)
            total = jnp.sum(weight, axis=1, keepdims=True)
            summed = jnp.dot(weight.astype(bf16), vbuf[b, :, span], preferred_element_type=f32)
            merged = jnp.zeros((both, 2 * LANES), f32)
            for h in range(2 * LANES // HEAD):
                piece = slice(h * both, (h + 1) * both)
                merged = jnp.where(wide_lane // HEAD == h, summed[piece], merged)
                c = g * 2 + h // 2
                at = inner * 4 + h % 2
                stat = st[c, r, :both]
                stat = jnp.where(lane == at, largest[piece], stat)
                st[c, r, :both] = jnp.where(lane == at + 2, total[piece], stat)
            merged = merged.astype(bf16)
            for half in range(2):
                bv[g * 2 + half, r, inner * both : (inner + 1) * both, :] = merged[
                    :, half * LANES : (half + 1) * LANES
                ]
        if groups == 1 and b < seqs - 1:
            send_piece(b)
    kept = 4 * per
    kept = -(-kept // 8) * 8
    for c in range(cols):
        for r in range(groups):
            st_part[c, r] = jnp.transpose(st[c, r])[:kept]
    st_copies = []
    for k, to in enumerate(peers):
        c, r = to // groups, lax.rem(to, groups)
        st_copies.append(remote(st_part.at[c, r], st_recv.at[k], st_s.at[k], st_r.at[k], "kv", to))
        st_copies[k].start()
    send_piece(pieces - 1)

    own = kv_part[me].astype(f32)
    for k in range(n - 1):
        kv_copies[k].wait()
        own = own + kv_recv[k].astype(f32)
    own = (own * factor).astype(bf16)
    kv_ref[me] = own
    query = q_all[me].astype(f32)
    spread = jnp.concatenate(
        [jnp.where(lane // QK == i, query, 0.0) for i in range(4)], axis=0
    ).astype(bf16)
    scores = lax.dot_general(
        spread, own[:, :LANES], (((1,), (1,)), ((), ())), preferred_element_type=f32
    )
    scores = jnp.where(lineage, scores * scale, masked_low)
    top = jnp.max(scores, axis=1, keepdims=True)
    weight = jnp.where(lineage, jnp.exp(scores - top), 0.0)
    total = jnp.sum(weight, axis=1, keepdims=True)
    summed = jnp.dot(weight.astype(bf16), own[:, LANES:], preferred_element_type=f32)

    def laid(array):
        found = []
        for b in range(per):
            for m in range(2):
                s0 = slice(m * part + b * prop, m * part + (b + 1) * prop)
                s1 = slice((2 + m) * part + b * prop, (2 + m) * part + (b + 1) * prop)
                found.append(jnp.where(low, array[s0], array[s1]))
        return jnp.concatenate(found, axis=0)

    tops, totals, sums = [laid(top)], [laid(total)], [laid(summed)]

    def take(stats, values):
        for which, into in ((0, tops), (2, totals)):
            into.append(
                jnp.concatenate(
                    [
                        jnp.where(
                            low,
                            stats[:both, b * 4 + which : b * 4 + which + 1],
                            stats[:both, b * 4 + which + 1 : b * 4 + which + 2],
                        )
                        for b in range(per)
                    ],
                    axis=0,
                )
            )
        sums.append(values.astype(f32))

    col, row = me // groups, lax.rem(me, groups)
    take(st[col, row], bv[col, row])
    filler = jnp.zeros((LANES - kept, LANES), f32)
    for copy in st_copies + b_copies:
        copy.wait()
    for k in range(n - 1):
        take(jnp.transpose(jnp.concatenate([st_recv[k], filler], axis=0)), bv_recv[k])
    highest = functools.reduce(jnp.maximum, tops)
    denominator = jnp.zeros_like(highest)
    numerator = jnp.zeros_like(highest)
    for a, b, c in zip(tops, totals, sums):
        share = jnp.exp(a - highest)
        denominator = denominator + b * share
        numerator = numerator + c * share
    attended = numerator / denominator
    heads = iota(lam_ref.shape, 1)
    lam_low = jnp.sum(jnp.where(heads == 2 * col, lam_ref[...], 0.0), axis=1, keepdims=True)
    lam_high = jnp.sum(jnp.where(heads == 2 * col + 1, lam_ref[...], 0.0), axis=1, keepdims=True)
    lam = jnp.where(low, lam_low, lam_high)
    gain = out_gain_ref[:, pl.ds(pl.multiple_of(col * LANES, LANES), LANES)]
    difference = jnp.concatenate(
        [
            attended[b * both : b * both + prop] - lam * attended[b * both + prop : (b + 1) * both]
            for b in range(per)
        ],
        axis=0,
    )
    squared = difference * difference
    one = jnp.sum(jnp.where(low, squared, 0.0), axis=1, keepdims=True)
    two = jnp.sum(jnp.where(low, 0.0, squared), axis=1, keepdims=True)
    mean = jnp.where(low, one, two) / HEAD
    norm_all[me] = (difference * lax.rsqrt(mean + epsilon) * gain).astype(bf16)
    gathers, late = [], []
    for k, to in enumerate(peers):
        gathers.append(remote(norm_all.at[me], norm_all.at[me], g_s.at[k], g_r.at[k], "kv", to))
        late.append(remote(kv_ref.at[me], kv_ref.at[me], ka_s.at[k], ka_r.at[k], "kv", to))
    for copy in gathers + late:
        copy.start()
    weights[3].wait()
    for copy in gathers:
        copy.wait()
    normed = jnp.concatenate(
        [
            jnp.concatenate([norm_all[c * groups + r] for r in range(groups)], axis=0)
            for c in range(cols)
        ],
        axis=1,
    )
    out_part[...] = jnp.dot(normed, wo_buf[...], preferred_element_type=f32).astype(bf16)
    copies = []
    for k in range(1, t):
        to = lax.rem(mine + k, t)
        copies.append(remote(out_part, out_recv.at[k], t_s.at[k], t_r.at[k], "tp", to))
    for copy in copies:
        copy.start()
    mixed = out_part[...].astype(f32)
    for k in range(1, t):
        copies[k - 1].wait()
        mixed = mixed + out_recv[k].astype(f32)
    out_ref[...] = mixed.astype(bf16)
    for copy in late:
        copy.wait()


def place_kernel(
    groups, prop, len_ref, acc_ref, kv_ref, keys_hbm, vals_hbm, nk_hbm, nv_hbm,
    kbuf, vbuf, k_in, v_in, k_out, v_out,
):
    seqs, length, width = kbuf.shape
    cols = width // LANES
    per = seqs // groups
    offset = lax.axis_index("kv") * length
    loads = []
    for b in range(seqs):
        loads.append(pltpu.make_async_copy(keys_hbm.at[b], kbuf.at[b], k_in.at[b]))
        loads.append(pltpu.make_async_copy(vals_hbm.at[b], vbuf.at[b], v_in.at[b]))
    for copy in loads:
        copy.start()
    stores = []
    window = 48
    for b in range(seqs):
        r, begin = b // per, (b % per) * prop
        rel = len_ref[b] + acc_ref[b] - offset
        base = jnp.clip((rel // 16) * 16, 0, length - window)
        at = pl.ds(pl.multiple_of(base, 16), window)
        slot = iota((window, prop), 0) + base - rel
        placing = (slot == iota((window, prop), 1)).astype(bf16)
        slot_col = iota((window, 1), 0) + base - rel
        inside = (slot_col >= 0) & (slot_col < prop)
        for which, buf in enumerate((kbuf, vbuf)):
            fresh = jnp.concatenate(
                [
                    kv_ref[c * groups + r, begin : begin + prop, which * LANES : (which + 1) * LANES]
                    for c in range(cols)
                ],
                axis=1,
            )
            moved = jnp.dot(placing, fresh, preferred_element_type=f32)
            loads[2 * b + which].wait()
            old = buf[b, at, :].astype(f32)
            buf[b, at, :] = jnp.where(inside, moved, old).astype(bf16)
            into, sem = ((nk_hbm, k_out), (nv_hbm, v_out))[which]
            stores.append(pltpu.make_async_copy(buf.at[b], into.at[b], sem.at[b]))
            stores[-1].start()
    for copy in stores:
        copy.wait()


def local(
    n, t, tokens, norm_gain, w_query, w_key, w_value, w_output, cache_keys, cache_values,
    map_lambda, out_gain, parents, lengths, accepted,
):
    rows, depth = tokens.shape
    seqs, length, width = cache_keys.shape
    prop = rows // seqs
    both = 2 * prop
    cols = min(n, width // LANES)
    groups = n // cols
    part = rows // groups
    per = seqs // groups
    pieces = seqs if groups == 1 else 1
    kept = -(-4 * per // 8) * 8
    out_cols = w_output.shape[1]
    vmem = pl.BlockSpec(memory_space=pltpu.VMEM)
    smem = pl.BlockSpec(memory_space=pltpu.SMEM)
    hbm = pl.BlockSpec(memory_space=pl.ANY)
    dma = pltpu.SemaphoreType.DMA
    V = pltpu.VMEM
    mixed, gathered = pl.pallas_call(
        functools.partial(main_kernel, n, t, cols, seqs, prop, depth * n),
        name="attend",
        out_shape=(
            jax.ShapeDtypeStruct((rows, out_cols), bf16),
            jax.ShapeDtypeStruct((n, part, 2 * LANES), bf16),
        ),
        in_specs=[vmem] * 5 + [smem] * 2 + [hbm] * 6,
        out_specs=(vmem, vmem),
        scratch_shapes=[
            V((3, depth, width), bf16),
            V(w_output.shape, bf16),
            V(cache_keys.shape, bf16),
            V(cache_values.shape, bf16),
            V((n, part, LANES), bf16),
            V((n, part, LANES), bf16),
            V((n, part, LANES), bf16),
            V((n, part, 2 * LANES), bf16),
            V((n, part, 2 * LANES), bf16),
            V((8, LANES), f32),
            V((n, 8, LANES), f32),
            V((cols, groups, per * both, LANES), bf16),
            V((n, per * both, LANES), bf16),
            V((cols, groups, LANES, LANES), f32),
            V((cols, groups, kept, LANES), f32),
            V((n, kept, LANES), f32),
            V((n, part, LANES), bf16),
            V((rows, out_cols), bf16),
            V((t, rows, out_cols), bf16),
            dma((4,)),
            dma((seqs,)),
            dma((seqs,)),
        ]
        + [dma((n,))] * 10
        + [dma((n, pieces))] * 2
        + [dma((n,))] * 4
        + [dma((t,))] * 2,
        compiler_params=pltpu.CompilerParams(collective_id=0, has_side_effects=True),
    )(
        tokens, norm_gain[None], map_lambda[None], out_gain[None], parents, lengths, accepted,
        w_query, w_key, w_value, w_output, cache_keys, cache_values,
    )
    new_keys, new_values = pl.pallas_call(
        functools.partial(place_kernel, groups, prop),
        name="place",
        out_shape=(
            jax.ShapeDtypeStruct(cache_keys.shape, bf16),
            jax.ShapeDtypeStruct(cache_values.shape, bf16),
        ),
        in_specs=[smem, smem, vmem, hbm, hbm],
        out_specs=(hbm, hbm),
        scratch_shapes=[V(cache_keys.shape, bf16), V(cache_values.shape, bf16)]
        + [dma((seqs,))] * 4,
    )(lengths, accepted, gathered, cache_keys, cache_values)
    return (mixed, new_keys, new_values)


def solution(mesh):
    placed = (
        P(None, "kv"),
        P("kv"),
        P("kv", "tp"),
        P("kv", "tp"),
        P("kv", "tp"),
        P("tp", "kv"),
        P(None, "kv", "tp"),
        P(None, "kv", "tp"),
        P("tp"),
        P("tp"),
        P(),
        P(),
        P(),
    )
    return jax.shard_map(
        functools.partial(local, mesh.shape["kv"], mesh.shape["tp"]),
        mesh=mesh,
        in_specs=placed,
        out_specs=(P(None, "kv"), P(None, "kv", "tp"), P(None, "kv", "tp")),
        check_vma=False,
    )
```

time: 87.4 us -> 64 us (0.73)
  the two profiles are of different devices: /device:TPU:1 before, /device:TPU:11 now
where the time goes in v2:
time: 64 us; the launch traced here: 63.8 us
  Pallas kernels  62.5 us (98%)
  between operations  0.67 us (1%)
  local copies, waits for them, and re-layouts  0.65 us (1%)
    pallas_call x1, Pallas kernels, local(): pl.pallas_call(functools.partial(main_kernel, n, t, cols, seqs, prop, dep...  54.9 us
    pallas_call x1, Pallas kernels, local(): pl.pallas_call(functools.partial(place_kernel, groups, prop), name='place...  7.54 us

profile of v2, /device:TPU:11, one launch (start us, length us, event | category | flops | bytes accessed | tf_op | source)
XLA Modules:
  0.0 63.8 jit_solution(7676920209433606589)
XLA Ops:
  0.6 54.9 %attend.1 = (bf16[96,512]{1,0:T(8,128)(2,1)}, bf16[8,96,256]{2,1,0:T(8,128)(2,1)}) custom-call(bf16[96,512]{1,0:T(8,128)(2,1)} %tok_ref.1, f32[1,512]{1,0:T(1,128)} %bitcast.4, f32[1,16]{1,0:T(1,128)} %bitcast.5, f32[1,1024]{1,0:T(1,128)} %bitcast.3, s32[4,24]{1,0:T(4,128)} %parent_ref.1, s32[4]{0:T(128)} %len_ref.3, s32[4]{0:T(128)} %acc_ref.3, ...), custom_call_target="tpu_custom_call" | custom-call | tf_op jit(solution)/shard_map/attend/pallas_call | solution.py:400
  55.6 0.0 copy-start
  55.6 7.5 %place.1 = (bf16[4,512,1024]{2,1,0:T(8,128)(2,1)}, bf16[4,512,1024]{2,1,0:T(8,128)(2,1)}) custom-call(s32[4]{0:T(128)} %len_ref.3, s32[4]{0:T(128)} %acc_ref.3, bf16[8,96,256]{2,1,0:T(8,128)(2,1)} %get-tuple-element.8.kv_ref, bf16[4,512,1024]{2,1,0:T(8,128)(2,1)} %keys_hbm.3, bf16[4,512,1024]{2,1,0:T(8,128)(2,1)} %vals_hbm.3), custom_call_target="tpu_custom_call" | custom-call | tf_op jit(solution)/shard_map/place/pallas_call | solution.py:442
  63.1 0.0 copy-done
  63.1 0.6 %copy.17 = bf16[96,512]{1,0:T(8,128)(2,1)} copy(bf16[96,512]{1,0:T(8,128)(2,1)S(1)} %copy-done) | data formatting | bytes 196608
Async XLA Ops:
  55.6 7.6 %copy-start = (bf16[96,512]{1,0:T(8,128)(2,1)S(1)}, bf16[96,512]{1,0:T(8,128)(2,1)}, u32[]{:S(2)}) copy-start(bf16[96,512]{1,0:T(8,128)(2,1)} %get-tuple-element.14) | copy-start | bytes 294916

commit v3 on v2

--- a/solution.py
+++ b/solution.py
@@ -1,4 +1,5 @@
 import functools
+import math
 
 import jax
 import jax.numpy as jnp
@@ -50,9 +51,9 @@
     tok_ref, gain_ref, lam_ref, out_gain_ref, parent_ref, len_ref, acc_ref,
     wq_hbm, wk_hbm, wv_hbm, wo_hbm, keys_hbm, vals_hbm,
     out_ref, kv_ref,
-    wbuf, wo_buf, kbuf, vbuf, q_part, q_recv, q_all, kv_part, kv_recv, sq_part, sq_recv,
+    wbuf, wo_buf, kbuf, vbuf, q_part, q_recv, q_all, kv_part, kvx_recv, kv_sum, kvz_recv, sq_part, sq_recv,
     bv, bv_recv, st, st_part, st_recv, norm_all, out_part, out_recv,
-    w_in, k_in, v_in, sq_s, sq_r, q_s, q_r, qa_s, qa_r, kv_s, kv_r, ka_s, ka_r,
+    w_in, k_in, v_in, sq_s, sq_r, q_s, q_r, qa_s, qa_r, kx_s, kx_r, kz_s, kz_r, ax_s, ax_r, az_s, az_r,
     b_s, b_r, st_s, st_r, g_s, g_r, t_s, t_r,
 ):
     me = lax.axis_index("kv")
@@ -65,6 +66,11 @@
     _, length, width = kbuf.shape
     scale = QK ** (-0.5)
     peers = [lax.rem(me + k, n) for k in range(1, n)]
+    inner_n = kv_ref.shape[0]
+    outer_n = n // inner_n
+    x, z = lax.rem(me, inner_n), me // inner_n
+    x_peers = [lax.rem(x + k, inner_n) for k in range(1, inner_n)]
+    z_peers = [lax.rem(z + k, outer_n) for k in range(1, outer_n)]
     barrier, count = greet((("kv", n), ("tp", t)))
     weights = [
         pltpu.make_async_copy(src, dst, w_in.at[i])
@@ -86,16 +92,26 @@
     sq_part[...] = jnp.broadcast_to(as_row, sq_part.shape)
     gained = (wide * gain_ref[...]).astype(bf16)
 
-    def products(which, into, at):
+    def products(which, place):
         weights[which].wait()
         product = jnp.dot(gained, wbuf[which], preferred_element_type=f32)
         for c in range(cols):
             for r in range(groups):
-                into[c * groups + r, :, at : at + LANES] = product[
-                    r * part : (r + 1) * part, c * LANES : (c + 1) * LANES
-                ].astype(bf16)
-
-    products(0, q_part, 0)
+                place(
+                    c * groups + r,
+                    product[r * part : (r + 1) * part, c * LANES : (c + 1) * LANES].astype(bf16),
+                )
+
+    def place_q(d, piece):
+        q_part[d] = piece
+
+    def place_k(d, piece):
+        kv_part[d % inner_n, d // inner_n, :, :LANES] = piece
+
+    def place_v(d, piece):
+        kv_part[d % inner_n, d // inner_n, :, LANES:] = piece
+
+    products(0, place_q)
     pl.semaphore_wait(barrier, count)
     sq_copies, q_copies = [], []
     for k, to in enumerate(peers):
@@ -103,8 +119,14 @@
         q_copies.append(remote(q_part.at[to], q_recv.at[k], q_s.at[k], q_r.at[k], "kv", to))
     for copy in sq_copies + q_copies:
         copy.start()
-    products(1, kv_part, 0)
-    products(2, kv_part, LANES)
+    products(1, place_k)
+    products(2, place_v)
+    kx_copies = [
+        remote(kv_part.at[to], kvx_recv.at[k], kx_s.at[k], kx_r.at[k], "kv", z * inner_n + to)
+        for k, to in enumerate(x_peers)
+    ]
+    for copy in kx_copies:
+        copy.start()
     squares = sq_part[...]
     for k in range(n - 1):
         sq_copies[k].wait()
@@ -118,11 +140,24 @@
         q_copies[k].wait()
         total = total + q_recv[k].astype(f32)
     q_all[me] = (total * factor).astype(bf16)
-    gathers, kv_copies = [], []
-    for k, to in enumerate(peers):
-        gathers.append(remote(q_all.at[me], q_all.at[me], qa_s.at[k], qa_r.at[k], "kv", to))
-        kv_copies.append(remote(kv_part.at[to], kv_recv.at[k], kv_s.at[k], kv_r.at[k], "kv", to))
-    for copy in gathers + kv_copies:
+    gathers = [
+        remote(q_all.at[me], q_all.at[me], qa_s.at[k], qa_r.at[k], "kv", to)
+        for k, to in enumerate(peers)
+    ]
+    for copy in gathers:
+        copy.start()
+    for copy in kx_copies:
+        copy.wait()
+    for i in range(outer_n):
+        summed = kv_part[x, i].astype(f32)
+        for k in range(inner_n - 1):
+            summed = summed + kvx_recv[k, i].astype(f32)
+        kv_sum[i] = summed.astype(bf16)
+    kz_copies = [
+        remote(kv_sum.at[to], kvz_recv.at[k], kz_s.at[k], kz_r.at[k], "kv", to * inner_n + x)
+        for k, to in enumerate(z_peers)
+    ]
+    for copy in kz_copies:
         copy.start()
 
     lane = iota((1, LANES), 1)
@@ -222,12 +257,18 @@
         st_copies[k].start()
     send_piece(pieces - 1)
 
-    own = kv_part[me].astype(f32)
-    for k in range(n - 1):
-        kv_copies[k].wait()
-        own = own + kv_recv[k].astype(f32)
+    own = kv_sum[z].astype(f32)
+    for k in range(outer_n - 1):
+        kz_copies[k].wait()
+        own = own + kvz_recv[k].astype(f32)
     own = (own * factor).astype(bf16)
-    kv_ref[me] = own
+    kv_ref[x, z] = own
+    az_copies = [
+        remote(kv_ref.at[x, z], kv_ref.at[x, z], az_s.at[k], az_r.at[k], "kv", to * inner_n + x)
+        for k, to in enumerate(z_peers)
+    ]
+    for copy in az_copies:
+        copy.start()
     query = q_all[me].astype(f32)
     spread = jnp.concatenate(
         [jnp.where(lane // QK == i, query, 0.0) for i in range(4)], axis=0
@@ -301,11 +342,19 @@
     two = jnp.sum(jnp.where(low, 0.0, squared), axis=1, keepdims=True)
     mean = jnp.where(low, one, two) / HEAD
     norm_all[me] = (difference * lax.rsqrt(mean + epsilon) * gain).astype(bf16)
-    gathers, late = [], []
-    for k, to in enumerate(peers):
-        gathers.append(remote(norm_all.at[me], norm_all.at[me], g_s.at[k], g_r.at[k], "kv", to))
-        late.append(remote(kv_ref.at[me], kv_ref.at[me], ka_s.at[k], ka_r.at[k], "kv", to))
-    for copy in gathers + late:
+    gathers = [
+        remote(norm_all.at[me], norm_all.at[me], g_s.at[k], g_r.at[k], "kv", to)
+        for k, to in enumerate(peers)
+    ]
+    for copy in gathers:
+        copy.start()
+    late = [
+        remote(kv_ref.at[x], kv_ref.at[x], ax_s.at[k], ax_r.at[k], "kv", z * inner_n + to)
+        for k, to in enumerate(x_peers)
+    ]
+    for copy in az_copies:
+        copy.wait()
+    for copy in late:
         copy.start()
     weights[3].wait()
     for copy in gathers:
@@ -340,6 +389,7 @@
     seqs, length, width = kbuf.shape
     cols = width // LANES
     per = seqs // groups
+    inner_n = kv_ref.shape[0]
     offset = lax.axis_index("kv") * length
     loads = []
     for b in range(seqs):
@@ -361,7 +411,12 @@
         for which, buf in enumerate((kbuf, vbuf)):
             fresh = jnp.concatenate(
                 [
-                    kv_ref[c * groups + r, begin : begin + prop, which * LANES : (which + 1) * LANES]
+                    kv_ref[
+                        (c * groups + r) % inner_n,
+                        (c * groups + r) // inner_n,
+                        begin : begin + prop,
+                        which * LANES : (which + 1) * LANES,
+                    ]
                     for c in range(cols)
                 ],
                 axis=1,
@@ -392,6 +447,8 @@
     pieces = seqs if groups == 1 else 1
     kept = -(-4 * per // 8) * 8
     out_cols = w_output.shape[1]
+    inner_n = math.gcd(n, 1 << (n.bit_length() - 1) // 2)
+    outer_n = n // inner_n
     vmem = pl.BlockSpec(memory_space=pltpu.VMEM)
     smem = pl.BlockSpec(memory_space=pltpu.SMEM)
     hbm = pl.BlockSpec(memory_space=pl.ANY)
@@ -402,7 +459,7 @@
         name="attend",
         out_shape=(
             jax.ShapeDtypeStruct((rows, out_cols), bf16),
-            jax.ShapeDtypeStruct((n, part, 2 * LANES), bf16),
+            jax.ShapeDtypeStruct((inner_n, outer_n, part, 2 * LANES), bf16),
         ),
         in_specs=[vmem] * 5 + [smem] * 2 + [hbm] * 6,
         out_specs=(vmem, vmem),
@@ -414,8 +471,10 @@
             V((n, part, LANES), bf16),
             V((n, part, LANES), bf16),
             V((n, part, LANES), bf16),
-            V((n, part, 2 * LANES), bf16),
-            V((n, part, 2 * LANES), bf16),
+            V((inner_n, outer_n, part, 2 * LANES), bf16),
+            V((inner_n, outer_n, part, 2 * LANES), bf16),
+            V((outer_n, part, 2 * LANES), bf16),
+            V((outer_n, part, 2 * LANES), bf16),
             V((8, LANES), f32),
             V((n, 8, LANES), f32),
             V((cols, groups, per * both, LANES), bf16),
@@ -430,7 +489,7 @@
             dma((seqs,)),
             dma((seqs,)),
         ]
-        + [dma((n,))] * 10
+        + [dma((n,))] * 14
         + [dma((n, pieces))] * 2
         + [dma((n,))] * 4
         + [dma((t,))] * 2,

time: 64 us -> 57.7 us (0.902)
  the two profiles are of different devices: /device:TPU:11 before, /device:TPU:1 now
where the time goes in v3:
time: 57.7 us; the launch traced here: 57.5 us
  Pallas kernels  56.2 us (97%)
  between operations  0.67 us (1%)
  local copies, waits for them, and re-layouts  0.65 us (1%)
    pallas_call x1, Pallas kernels, local(): pl.pallas_call(functools.partial(main_kernel, n, t, cols, seqs, prop, dep...  48.7 us
    pallas_call x1, Pallas kernels, local(): pl.pallas_call(functools.partial(place_kernel, groups, prop), name='place...  7.54 us

profile of v3, /device:TPU:1, one launch (start us, length us, event | category | flops | bytes accessed | tf_op | source)
XLA Modules:
  0.0 57.5 jit_solution(6195288257042874457)
XLA Ops:
  0.6 48.7 %attend.1 = (bf16[96,512]{1,0:T(8,128)(2,1)}, bf16[2,4,96,256]{3,2,1,0:T(8,128)(2,1)}) custom-call(bf16[96,512]{1,0:T(8,128)(2,1)} %tok_ref.1, f32[1,512]{1,0:T(1,128)} %bitcast.4, f32[1,16]{1,0:T(1,128)} %bitcast.5, f32[1,1024]{1,0:T(1,128)} %bitcast.3, s32[4,24]{1,0:T(4,128)} %parent_ref.1, s32[4]{0:T(128)} %len_ref.3, s32[4]{0:T(128)} %acc_ref.3, ...), custom_call_target="tpu_custom_call" | custom-call | tf_op jit(solution)/shard_map/attend/pallas_call | solution.py:457
  49.3 0.0 copy-start
  49.3 7.5 %place.1 = (bf16[4,512,1024]{2,1,0:T(8,128)(2,1)}, bf16[4,512,1024]{2,1,0:T(8,128)(2,1)}) custom-call(s32[4]{0:T(128)} %len_ref.3, s32[4]{0:T(128)} %acc_ref.3, bf16[2,4,96,256]{3,2,1,0:T(8,128)(2,1)} %get-tuple-element.8.kv_ref, bf16[4,512,1024]{2,1,0:T(8,128)(2,1)} %keys_hbm.3, bf16[4,512,1024]{2,1,0:T(8,128)(2,1)} %vals_hbm.3), custom_call_target="tpu_custom_call" | custom-call | tf_op jit(solution)/shard_map/place/pallas_call | solution.py:501
  56.9 0.0 copy-done
  56.9 0.6 %copy.17 = bf16[96,512]{1,0:T(8,128)(2,1)} copy(bf16[96,512]{1,0:T(8,128)(2,1)S(1)} %copy-done) | data formatting | bytes 196608
Async XLA Ops:
  49.3 7.6 %copy-start = (bf16[96,512]{1,0:T(8,128)(2,1)S(1)}, bf16[96,512]{1,0:T(8,128)(2,1)}, u32[]{:S(2)}) copy-start(bf16[96,512]{1,0:T(8,128)(2,1)} %get-tuple-element.14) | copy-start | bytes 294916
